TPU v7x, 32 devices: a whole 2x2x4 slice. The times are simulated.
32 devices in a mesh: sp: 4 (over z), tp: 8 (over y, x, core).
Axes of the slice: x: 2, y: 2, z: 4, core: 2. Of those that a mesh axis runs over, the one named last changes fastest.
Arguments:
- context_activations: bfloat16 [2, 1024, 4096], P(None, 'sp', 'tp'), may hold values from -6 to 6
- first_generated_activation: bfloat16 [2, 4096], replicated, may hold values from -6 to 6
- address_projection: bfloat16 [4096, 1024], P(None, 'tp'), may hold values from -0.09375 to 0.09375
- payload_projection: bfloat16 [4096, 1024], P(None, 'tp'), may hold values from -0.09375 to 0.09375
- lookup_projection: bfloat16 [4096, 1024], P(None, 'tp'), may hold values from -0.09375 to 0.09375
- exit_gating_projection: bfloat16 [4096, 1024], P(None, 'tp'), may hold values from -0.09375 to 0.09375
- writing_intensity_projection: bfloat16 [4096, 8], replicated, may hold values from -0.09375 to 0.09375
- fading_projection: bfloat16 [4096, 8], replicated, may hold values from -0.09375 to 0.09375
- channel_fading_speed: float32 [8], replicated, may hold values from 0 to 1, as said below
- extra_fading_log: float32 [2, 1024, 8], P(None, 'sp', 'tp'), may hold values from -1 to 0, as said below
- readout_normalizer_gain: float32 [128], replicated, may hold values from 0.1 to 1.9
- exit_projection: bfloat16 [1024, 4096], P('tp'), may hold values from -0.1875 to 0.1875
Outputs:
- state_cache: bfloat16 [2, 4, 8, 128, 128], P(None, 'sp', 'tp')
- step_out: bfloat16 [2, 4096], P(None, 'tp')
Inputs may be any that keep to these rules, and one draw needn't show every extreme that they name: `channel_fading_speed`: positive rates, one a head. `extra_fading_log`: zero at all but a few positions of each prompt and head, negative there.
All inputs are finite; a program needn't handle non-finite values.
Results may differ from a plain program's by a relative error of at most 0.012.
Values may be sent and summed in bfloat16 or wider, within the bound.
A program may use at most 64 MiB of HBM per device.

v0:
```python
import jax
import jax.numpy as jnp
from jax import lax
from jax.sharding import PartitionSpec as P

BLOCK = 64
norm_eps = 1e-06
highest = lax.Precision.HIGHEST


def carried_in(value, axis, combine, identity):
    devices, position = (lax.axis_size(axis), lax.axis_index(axis))
    everything = jax.tree.map(
        lambda part, kind: lax.all_gather(part.astype(kind), axis),
        value,
        (jnp.bfloat16, jnp.bfloat16),
    )
    start = jax.tree.map(
        lambda part, zero: jnp.broadcast_to(jnp.asarray(zero, part.dtype), part.shape),
        value,
        identity,
    )

    def lap(k, before):
        reached = k < position
        new = combine(
            before, jax.tree.map(lambda part, own: part[k].astype(own.dtype), everything, value)
        )
        return jax.tree.map(lambda a, b: jnp.where(reached, a, b), new, before)

    return lax.fori_loop(0, devices, lap, start)


def carried_in_2(value, axis, combine, identity):
    devices, position = (lax.axis_size(axis), lax.axis_index(axis))
    everything = lax.all_gather(value, axis)
    start = jnp.broadcast_to(jnp.asarray(identity, value.dtype), value.shape)

    def lap(k, before):
        at = devices - 1 - k
        reached = at > position
        new = combine(before, everything[at])
        return jnp.where(reached, new, before)

    return lax.fori_loop(0, devices, lap, start)


def unit_rows(values_in):
    return values_in * lax.rsqrt(jnp.sum(values_in * values_in, axis=-1, keepdims=True) + norm_eps)


def compose(left, right):
    return jnp.einsum("...ij,...jk->...ik", left, right, precision=highest)


def segment_map(keys_in, values_in, beta_gate, fading_exponent):
    blocks = keys_in.shape[0] // BLOCK
    key_blocks = keys_in.reshape(blocks, BLOCK, -1)
    value_blocks = values_in.reshape(blocks, BLOCK, -1)
    beta_blocks = beta_gate.reshape(blocks, BLOCK)
    cumul = jnp.cumsum(fading_exponent.reshape(blocks, BLOCK), axis=-1)
    causal = jnp.tril(jnp.ones((BLOCK, BLOCK), bool))
    strict = jnp.tril(jnp.ones((BLOCK, BLOCK), bool), -1)
    gaps_log = cumul[:, :, None] - cumul[:, None, :]
    within = jnp.where(causal, jnp.exp(jnp.where(causal, gaps_log, 0.0)), 0.0)
    keys_beta = key_blocks * beta_blocks[..., None]
    strict_part = jnp.where(
        strict, jnp.einsum("nid,njd->nij", keys_beta, key_blocks, precision=highest) * within, 0.0
    )
    targets = jnp.concatenate(
        [value_blocks * beta_blocks[..., None], keys_beta * jnp.exp(cumul)[..., None]], axis=-1
    )
    system = jnp.eye(BLOCK, dtype=jnp.float32) + strict_part
    solved = lax.linalg.triangular_solve(system, targets, left_side=True, lower=True)
    width_v = value_blocks.shape[-1]
    width_k = key_blocks.shape[-1]
    pseudo_values = solved[..., :width_v]
    decayed_keys = solved[..., width_v:]
    carried_values = jnp.concatenate(
        [jnp.zeros((blocks, BLOCK, width_k), jnp.float32), pseudo_values], axis=-1
    )
    trailing = key_blocks * jnp.exp(cumul[:, -1:] - cumul)[..., None]
    block_decay = jnp.exp(cumul[:, -1])

    def advance(memory, inputs):
        pseudo, decayed, trail_keys, shrink = inputs
        fresh_values = pseudo - jnp.dot(decayed, memory, precision=highest)
        memory = memory * shrink + jnp.dot(trail_keys.T, fresh_values, precision=highest)
        return (memory, None)

    start_map = jnp.concatenate(
        [jnp.eye(width_k, dtype=jnp.float32), jnp.zeros((width_k, width_v), jnp.float32)], axis=1
    )
    memory, _ = lax.scan(advance, start_map, (carried_values, decayed_keys, trailing, block_decay))
    return memory


def combine_maps(earlier, later):
    return (compose(later[0], earlier[0]), compose(later[0], earlier[1]) + later[1])


def body(
    context_activations,
    first_generated_activation,
    address_projection,
    payload_projection,
    lookup_projection,
    exit_gating_projection,
    writing_intensity_projection,
    fading_projection,
    channel_fading_speed,
    extra_fading_log,
    readout_normalizer_gain,
    exit_projection,
):
    head_size = readout_normalizer_gain.shape[0]
    current_heads = address_projection.shape[1] // head_size
    first_head = lax.axis_index("tp") * current_heads
    beta_cols = lax.dynamic_slice_in_dim(writing_intensity_projection, first_head, current_heads, 1)
    decay_cols = lax.dynamic_slice_in_dim(fading_projection, first_head, current_heads, 1)
    logit_weight = jnp.concatenate([beta_cols, decay_cols], axis=1)
    fading_speeds = lax.dynamic_slice_in_dim(channel_fading_speed, first_head, current_heads, 0)
    seq_count, length = (context_activations.shape[0], context_activations.shape[1])
    portion = lax.all_gather(context_activations, "tp", axis=2, tiled=True)
    key_sum = jnp.einsum(
        "abf,fc->abc", portion, address_projection, preferred_element_type=jnp.float32
    )
    value_sum = jnp.einsum(
        "abf,fc->abc", portion, payload_projection, preferred_element_type=jnp.float32
    )
    logit_sum = jnp.einsum("abf,fc->abc", portion, logit_weight, preferred_element_type=jnp.float32)
    shaped = (seq_count, length, current_heads, head_size)
    keys_here = unit_rows(jax.nn.silu(key_sum).reshape(shaped)).astype(jnp.bfloat16)
    values_here = jax.nn.silu(value_sum).reshape(shaped).astype(jnp.bfloat16)
    current_scores = logit_sum.astype(jnp.bfloat16)
    beta_gate = jax.nn.sigmoid(current_scores[..., :current_heads].astype(jnp.float32))
    fading_exponent = extra_fading_log - fading_speeds * jax.nn.softplus(
        current_scores[..., current_heads:].astype(jnp.float32)
    )
    maps = jax.vmap(jax.vmap(segment_map, in_axes=(1, 1, 1, 1)))(
        keys_here.astype(jnp.float32), values_here.astype(jnp.float32), beta_gate, fading_exponent
    )
    own_moves = maps[..., :head_size]
    own_offset = maps[..., head_size:]
    heads_shape = (seq_count, current_heads, head_size)
    new_keys = unit_rows(
        jax.nn.silu(
            jnp.dot(
                first_generated_activation, address_projection, preferred_element_type=jnp.float32
            )
        ).reshape(heads_shape)
    )
    new_values = jax.nn.silu(
        jnp.dot(first_generated_activation, payload_projection, preferred_element_type=jnp.float32)
    ).reshape(heads_shape)
    new_queries = unit_rows(
        jax.nn.silu(
            jnp.dot(
                first_generated_activation, lookup_projection, preferred_element_type=jnp.float32
            )
        ).reshape(heads_shape)
    )
    out_gate = jax.nn.silu(
        jnp.dot(
            first_generated_activation, exit_gating_projection, preferred_element_type=jnp.float32
        )
    ).reshape(heads_shape)
    new_logits = jnp.dot(
        first_generated_activation, logit_weight, preferred_element_type=jnp.float32
    )
    new_beta = jax.nn.sigmoid(new_logits[:, :current_heads])
    new_decay = jnp.exp(-fading_speeds * jax.nn.softplus(new_logits[:, current_heads:]))
    intersection_kq = jnp.sum(new_keys * new_queries, axis=-1, keepdims=True)
    carried_query = new_decay[..., None] * (
        new_queries - new_beta[..., None] * new_keys * intersection_kq
    )
    own_write = new_beta[..., None] * new_values * intersection_kq
    identity = jnp.broadcast_to(jnp.eye(head_size, dtype=jnp.float32), own_moves.shape)
    prefix_moves, prefix_offset = carried_in(
        (own_moves, own_offset), "sp", combine_maps, (identity, jnp.zeros_like(own_offset))
    )
    states_here = compose(own_moves, prefix_offset) + own_offset

    def chain_later(earlier, later):
        return compose(earlier, later)

    later_moves = carried_in_2(own_moves, "sp", chain_later, identity)
    lifted = jnp.einsum("shjk,shj->shk", later_moves, carried_query, precision=highest)
    term = jnp.einsum("shk,shkv->shv", lifted, own_offset, precision=highest)
    read = lax.psum(term, "sp") + own_write
    state_cache = states_here.astype(jnp.bfloat16)[:, None]
    normed = (
        read
        * lax.rsqrt(jnp.mean(read * read, axis=-1, keepdims=True) + norm_eps)
        * readout_normalizer_gain
        * out_gate
    )
    normed = normed.astype(jnp.bfloat16).reshape(seq_count, current_heads * head_size)
    partial_out = jnp.dot(normed, exit_projection, preferred_element_type=jnp.float32)
    step_out = lax.psum_scatter(partial_out, "tp", scatter_dimension=1, tiled=True).astype(
        jnp.bfloat16
    )
    return (state_cache, step_out)


def solution(mesh):
    placed = (
        P(None, "sp", "tp"),
        P(),
        P(None, "tp"),
        P(None, "tp"),
        P(None, "tp"),
        P(None, "tp"),
        P(),
        P(),
        P(),
        P(None, "sp", "tp"),
        P(),
        P("tp", None),
    )
    return jax.shard_map(
        body,
        mesh=mesh,
        in_specs=placed,
        out_specs=(P(None, "sp", "tp", None, None), P(None, "tp")),
        check_vma=False,
    )
```

profile of v0, /device:TPU:0, one launch (start us, length us, event | category | flops | bytes accessed | tf_op | source)
XLA Modules:
  0.0 188.7 jit_solution(4630512967896987474)
XLA Ops:
  7.2 0.7 all-gather.5.cloned.1.call-update
  8.1 1.3 dynamic_slice.48
  10.2 1.6 multiply_reduce_fusion.4
  11.8 1.1 multiply_reduce_fusion.3
  12.9 0.2 multiply_reduce_fusion.2
  13.1 0.9 constant_dynamic-slice_fusion.1
  14.0 0.9 convolution_bitcast_fusion.6
  15.1 34.9 %all-gather.5.cloned.1.call-done = bf16[2,256,4096]{2,1,0:T(8,128)(2,1)} async-done(((bf16[2,256,512]{2,1,0:T(8,128)(2,1)}), bf16[2,256,4096]{2,1,0:T(8,128)(2,1)}) %all-gather.5.cloned.1.call-update) | async-done | bytes 4194320 | tf_op jit(solution)/shard_map/all_gather | solution.py:124
  50.0 3.4 %fusion.31 = bf16[2,256,2]{1,2,0:T(2,128)(2,1)S(1)} fusion(bf16[2,256,4096]{2,1,0:T(8,128)(2,1)} %all-gather.5.cloned.1.call-done, bf16[4096,1]{0,1:T(2,128)(2,1)S(1)} %get-tuple-element.365, bf16[4096,1]{0,1:T(2,128)(2,1)S(1)} %get-tuple-element.366), kind=kOutput, calls=%fused_computation.41 | convolution fusion | flops 8422400 | bytes 4212736 | tf_op jit(solution)/shard_map/abf,fc->abc/dot_general | solution.py:131
  53.3 0.7 fusion.63
  54.2 0.5 reduce_window_sum.11
  54.7 0.2 slice_reduce_fusion
  55.0 3.6 %multiply_reduce_fusion = (f32[2,256]{1,0:T(2,128)S(1)}, f32[2,256,128]{2,1,0:T(8,128)S(1)}) fusion(bf16[2,256,4096]{2,1,0:T(8,128)(2,1)} %all-gather.5.cloned.1.call-done, bf16[4096,128]{1,0:T(8,128)(2,1)S(1)} %copy-done), kind=kOutput, calls=%fused_computation.60 | convolution fusion | flops 537263616 | bytes 5507072 | tf_op jit(solution)/shard_map/abf,fc->abc/dot_general | solution.py:125
  58.7 0.4 fusion.27
  59.1 39.3 %custom-call.3 = f32[2,1,4,1,64,64]{4,5,3,2,1,0:T(8,128)S(1)} custom-call(f32[2,1,4,1,64,64]{5,4,3,2,1,0:T(8,128)S(1)} %fusion.27), custom_call_target="InvertDiagBlocksLowerTriangular" | custom-call | tf_op jit(solution)/shard_map/vmap(vmap())/triangular_solve | solution.py:74
  98.5 3.5 %multiply_convert_fusion = bf16[2,256,128]{2,1,0:T(8,128)(2,1)S(1)} fusion(bf16[2,256,4096]{2,1,0:T(8,128)(2,1)} %all-gather.5.cloned.1.call-done, bf16[4096,128]{1,0:T(8,128)(2,1)S(1)} %copy-done.5), kind=kOutput, calls=%fused_computation.56 | convolution fusion | flops 537198592 | bytes 5373952 | tf_op jit(solution)/shard_map/abf,fc->abc/dot_general | solution.py:128
  101.9 0.3 multiply_multiply_fusion
  102.2 0.7 convolution_bitcast_fusion.3
  103.1 3.0 %while.39 = (s32[]{:T(128)}, f32[2,1,128,256]{3,2,0,1:T(8,128)S(1)}, f32[4,2,1]{1,2,0:T(1,128)S(1)}, f32[4,2,1,64,128]{4,3,0,1,2:T(8,128)S(1)}, f32[4,2,1,64,256...) while((s32[]{:T(128)}, f32[2,1,128,256]{3,2,0,1:T(8,128)S(1)}, ...), condition=%wide.region_3.4_spmd, body=%wide.region_2.3_spmd.sunk | while | flops 100827136 | bytes 1312357 | solution.py:94
  103.1 0.3 convolution_subtract_fusion.2
  103.4 0.4 fusion.110
  103.8 0.3 convolution_subtract_fusion.2
  104.1 0.4 fusion.110
  104.6 0.3 convolution_subtract_fusion.2
  104.9 0.4 fusion.110
  105.3 0.3 convolution_subtract_fusion.2
  105.6 0.4 fusion.110
  106.2 16.2 %all-gather.2 = f32[8,1,128,128]{3,2,1,0:T(8,128)S(1)} all-gather(f32[2,1,128,128]{3,2,1,0:T(8,128)S(1)} %slice_bitcast_fusion.1), channel_id=4, replica_groups=mesh['sp'=4,'tp'=8] {'sp'}, dimensions={0}, use_global_device_ids=true | all-gather | bytes 655360 | tf_op jit(solution)/shard_map/all_gather | solution.py:36
  122.4 1.8 while.40
  122.4 0.4 fusion.113
  122.9 0.4 fusion.113
  123.3 0.4 fusion.113
  123.8 0.4 fusion.113
  124.2 0.3 convolution_bitcast_fusion.5
  124.5 0.2 fusion.44
  124.7 12.1 %psum.7 = f32[2,1,128]{2,0,1:T(2,128)S(1)} all-reduce(f32[2,1,128]{2,0,1:T(2,128)S(1)} %bitcast.222), channel_id=1, replica_groups=mesh['sp'=4,'tp'=8] {'sp'}, use_global_device_ids=true, to_apply=%region_11.12 | all-reduce | flops 256 | bytes 2048 | tf_op jit(solution)/shard_map/psum | solution.py:190
  136.8 1.6 multiply_reduce_fusion.1
  138.5 3.3 %convolution_bitcast_fusion.2 = f32[4096,2]{1,0:T(8,128)} fusion(bf16[128,4096]{1,0:T(8,128)(2,1)S(1)} %copy-done.1, f32[2,1,128]{2,0,1:T(2,128)S(1)} %get-tuple-element.345, f32[128]{0:T(128)S(1)} %copy-done.4, f32[2]{0:T(128)S(1)} %add_rsqrt_fusion.1, bf16[2,4096]{1,0:T(2,128)(2,1)S(1)} %copy-done.2, bf16[4096,128]{1,0:T(8,128)(2,1)} %param.23), kind=kOutput, calls=%fused_computation.29 | convolution fusion | flops 4196352 | bytes 2147848
  141.8 14.4 %all-gather = bf16[8,1,128,128]{3,2,1,0:T(8,128)(2,1)S(1)} all-gather(bf16[2,1,128,128]{3,2,1,0:T(8,128)(2,1)S(1)} %get-tuple-element.355), channel_id=2, replica_groups=mesh['sp'=4,'tp'=8] {'sp'}, dimensions={0}, use_global_device_ids=true | all-gather | bytes 327680 | tf_op jit(solution)/shard_map/all_gather | solution.py:14
  156.2 13.8 %all-gather.1 = bf16[8,1,128,128]{3,2,1,0:T(8,128)(2,1)S(1)} all-gather(bf16[2,1,128,128]{3,2,1,0:T(8,128)(2,1)S(1)} %get-tuple-element.354), channel_id=3, replica_groups=mesh['sp'=4,'tp'=8] {'sp'}, dimensions={0}, use_global_device_ids=true | all-gather | bytes 327680 | tf_op jit(solution)/shard_map/all_gather | solution.py:14
  170.0 1.1 while.41
  170.0 0.2 fusion.116
  170.3 0.2 fusion.116
  170.6 0.2 fusion.116
  170.8 0.2 fusion.116
  171.1 0.9 fusion.30
  172.0 8.3 %reduce-scatter.4.cloned.1.call-done = f32[512,2]{1,0:T(8,128)} async-done(((f32[4096,2]{1,0:T(8,128)}), f32[512,2]{1,0:T(8,128)}) %reduce-scatter.4.cloned.1.call-update) | async-done | bytes 4112
  180.3 1.6 copy.60
  (50 shorter events, 1.2 us)
Async XLA Ops:
  7.2 4.6 %copy-start = (bf16[4096,128]{1,0:T(8,128)(2,1)S(1)}, bf16[4096,128]{1,0:T(8,128)(2,1)}, u32[]{:S(2)}) copy-start(bf16[4096,128]{1,0:T(8,128)(2,1)} %param.20) | copy-start | bytes 3145732
  7.2 46.2 %copy-start.3 = (f32[2,256,1]{1,2,0:T(1,128)S(1)}, f32[2,256,1]{1,2,0:T(1,128)}, u32[]{:S(2)}) copy-start(f32[2,256,1]{1,2,0:T(1,128)} %param.27) | copy-start | bytes 6148
  7.2 42.8 %all-gather.5.cloned.1.call-start = ((), (), s32[]{:S(2)}) async-start(), calls=%async_computation.1 | async-start | bytes 4718592 | tf_op jit(solution)/shard_map/all_gather | solution.py:124
  7.9 172.3 %reduce-scatter.4.cloned.1.call-start = ((), (), s32[]{:S(2)}) async-start(), calls=%async_computation.2 | async-start | bytes 2359296
  54.1 44.4 %copy-start.5 = (bf16[4096,128]{1,0:T(8,128)(2,1)S(1)}, bf16[4096,128]{1,0:T(8,128)(2,1)}, u32[]{:S(2)}) copy-start(bf16[4096,128]{1,0:T(8,128)(2,1)} %param.21) | copy-start | bytes 3145732
  106.1 30.8 %copy-start.2 = (bf16[2,4096]{1,0:T(2,128)(2,1)S(1)}, bf16[2,4096]{1,0:T(2,128)(2,1)}, u32[]{:S(2)}) copy-start(bf16[2,4096]{1,0:T(2,128)(2,1)} %param.19) | copy-start | bytes 49156
  106.1 32.4 %copy-start.1 = (bf16[128,4096]{1,0:T(8,128)(2,1)S(1)}, bf16[128,4096]{1,0:T(8,128)(2,1)}, u32[]{:S(2)}) copy-start(bf16[128,4096]{1,0:T(8,128)(2,1)} %param.29) | copy-start | bytes 3145732
  106.1 32.4 %copy-start.4 = (f32[128]{0:T(128)S(1)}, f32[128]{0:T(128)}, u32[]{:S(2)}) copy-start(f32[128]{0:T(128)} %param.28) | copy-start | bytes 1540
Sparse Core Ops, SparseCore 0:
  9.9 40.0 all-gather.4
  141.9 38.3 reduce-scatter.3
where the time goes:
time: 189 us
  blocking collectives  56.6 us (30%)
  waiting for transfers between devices  43.9 us (23%)
  other arithmetic  41.5 us (22%)
  matrix products  26.6 us (14%)
  between operations  15 us (8%)
  local copies, waits for them, and re-layouts  4.71 us (2%)
    another operation x1, other arithmetic, segment_map(): lax.linalg.triangular_solve(system, targets, left_side=True, lower=True)  39.3 us
    all_gather x1, waiting for transfers between devices, body(): portion = lax.all_gather(context_activations, 'tp', axis=2, tiled=True)  34.9 us
    all_gather x2, blocking collectives, carried_in(): lax.all_gather(part.astype(kind), axis)  28.2 us
    all_gather x1, blocking collectives, carried_in_2(): everything = lax.all_gather(value, axis)  16.2 us
    psum x1, blocking collectives, body(): read = lax.psum(term, 'sp') + own_write  12.1 us
    unnamed x3, waiting for transfers between devices  8.97 us
  transfers between devices with their start and end apart: 2, of which 2 were waited for; matrix products, arithmetic and copies ran while one was open for 4% of the time, Pallas kernels for 0%

commit v1 on v0

--- a/solution.py
+++ b/solution.py
@@ -121,7 +121,12 @@
     logit_weight = jnp.concatenate([beta_cols, decay_cols], axis=1)
     fading_speeds = lax.dynamic_slice_in_dim(channel_fading_speed, first_head, current_heads, 0)
     seq_count, length = (context_activations.shape[0], context_activations.shape[1])
-    portion = lax.all_gather(context_activations, "tp", axis=2, tiled=True)
+    ring = [context_activations]
+    for hop in range(7):
+        ring.append(lax.ppermute(ring[-1], "tp", [(dev, (dev + 1) % 8) for dev in range(8)]))
+    portion = jnp.roll(
+        jnp.concatenate(ring[::-1], axis=2), (lax.axis_index("tp") + 1) * ring[0].shape[2], axis=2
+    )
     key_sum = jnp.einsum(
         "abf,fc->abc", portion, address_projection, preferred_element_type=jnp.float32
     )

time: 189 us -> 222 us (1.17)
  waiting for transfers between devices: 43.9 us -> 67.6 us
  local copies, waits for them, and re-layouts: 4.71 us -> 16.4 us
  matrix products: 26.6 us -> 23.1 us
    ppermute x0 -> x7, waiting for transfers between devices: none -> 59 us  [body(): lax.ppermute(ring[-1], 'tp', [(dev, (dev + 1) % 8) for dev in range(8)])]
    all_gather x1 -> x0, waiting for transfers between devices: 34.9 us -> none  [body(): portion = lax.all_gather(context_activations, 'tp', axis=2, tiled=True)]
    unnamed x14 -> x35, local copies, waits for them, and re-layouts: 1.78 us -> 6.7 us
    mul x4, local copies, waits for them, and re-layouts: 0.04 us -> 2.65 us  [advance(): memory * shrink + jnp.dot(trail_keys.T, fresh_values, precision=highest)]
    unnamed x3 -> x2, waiting for transfers between devices: 8.97 us -> 8.52 us
  transfers between devices with their start and end apart: 2 -> 8, of which waited for: 2 -> 8; matrix products, arithmetic and copies ran while one was open for 4% -> 4% of each run, Pallas kernels for 0% -> 0%
where the time goes in v1:
time: 222 us; the launch traced here: 221 us
  waiting for transfers between devices  67.6 us (30%)
  blocking collectives  55.8 us (25%)
  other arithmetic  42 us (19%)
  matrix products  23.1 us (10%)
  local copies, waits for them, and re-layouts  16.4 us (7%)
  between operations  15.1 us (7%)
    ppermute x7, waiting for transfers between devices, body(): lax.ppermute(ring[-1], 'tp', [(dev, (dev + 1) % 8) for dev in range(8)])  59 us
    another operation x1, other arithmetic, segment_map(): lax.linalg.triangular_solve(system, targets, left_side=True, lower=True)  39.3 us
    all_gather x2, blocking collectives, carried_in(): lax.all_gather(part.astype(kind), axis)  28.1 us
    all_gather x1, blocking collectives, carried_in_2(): everything = lax.all_gather(value, axis)  15.8 us
    psum x1, blocking collectives, body(): read = lax.psum(term, 'sp') + own_write  11.8 us
    unnamed x2, waiting for transfers between devices  8.52 us
    unnamed x35, local copies, waits for them, and re-layouts  6.7 us
  transfers between devices with their start and end apart: 8, of which 8 were waited for; matrix products, arithmetic and copies ran while one was open for 4% of the time, Pallas kernels for 0%

profile of v1, /device:TPU:0, one launch (start us, length us, event | category | flops | bytes accessed | tf_op | source)
XLA Modules:
  0.0 221.0 jit_solution(9877608382965338271)
XLA Ops:
  7.2 0.5 collective-permute-start
  7.8 9.9 %collective-permute-done = bf16[2,256,512]{2,1,0:T(8,128)(2,1)S(1)} collective-permute-done((bf16[2,256,512]{2,1,0:T(8,128)(2,1)}, bf16[2,256,512]{2,1,0:T(8,128)(2,1)S(1)}, u32[]{:S(2)}, u32[]{:S(2)}) %collective-permute-start) | collective-permute-done | bytes 524320 | tf_op jit(solution)/shard_map/ppermute | solution.py:126
  17.7 9.5 %collective-permute-done.1 = bf16[2,256,512]{2,1,0:T(8,128)(2,1)S(1)} collective-permute-done((bf16[2,256,512]{2,1,0:T(8,128)(2,1)S(1)}, bf16[2,256,512]{2,1,0:T(8,128)(2,1)S(1)}, u32[]{:S(2)}, u32[]{:S(2)}) %collective-permute-start.1) | collective-permute-done | bytes 524320 | tf_op jit(solution)/shard_map/ppermute | solution.py:126
  27.2 1.6 multiply_reduce_fusion.4
  28.8 7.9 %collective-permute-done.2 = bf16[2,256,512]{2,1,0:T(8,128)(2,1)S(1)} collective-permute-done((bf16[2,256,512]{2,1,0:T(8,128)(2,1)S(1)}, bf16[2,256,512]{2,1,0:T(8,128)(2,1)S(1)}, u32[]{:S(2)}, u32[]{:S(2)}) %collective-permute-start.2) | collective-permute-done | bytes 524320 | tf_op jit(solution)/shard_map/ppermute | solution.py:126
  36.9 1.2 dynamic_slice.52
  38.8 0.7 concatenate.18.clone
  39.5 1.1 multiply_reduce_fusion.3
  40.6 5.8 %collective-permute-done.3 = bf16[2,256,512]{2,1,0:T(8,128)(2,1)} collective-permute-done((bf16[2,256,512]{2,1,0:T(8,128)(2,1)S(1)}, bf16[2,256,512]{2,1,0:T(8,128)(2,1)}, u32[]{:S(2)}, u32[]{:S(2)}) %collective-permute-start.3) | collective-permute-done | bytes 524320 | tf_op jit(solution)/shard_map/ppermute | solution.py:126
  46.5 0.9 constant_dynamic-slice_fusion.1
  47.5 8.6 %collective-permute-done.4 = bf16[2,256,512]{2,1,0:T(8,128)(2,1)S(1)} collective-permute-done((bf16[2,256,512]{2,1,0:T(8,128)(2,1)}, bf16[2,256,512]{2,1,0:T(8,128)(2,1)S(1)}, u32[]{:S(2)}, u32[]{:S(2)}) %collective-permute-start.4) | collective-permute-done | bytes 524320 | tf_op jit(solution)/shard_map/ppermute | solution.py:126
  56.1 0.9 convolution_bitcast_fusion.6
  57.0 8.6 %collective-permute-done.5 = bf16[2,256,512]{2,1,0:T(8,128)(2,1)S(1)} collective-permute-done((bf16[2,256,512]{2,1,0:T(8,128)(2,1)S(1)}, bf16[2,256,512]{2,1,0:T(8,128)(2,1)S(1)}, u32[]{:S(2)}, u32[]{:S(2)}) %collective-permute-start.5) | collective-permute-done | bytes 524320 | tf_op jit(solution)/shard_map/ppermute | solution.py:126
  65.6 0.7 subtract_multiply_fusion
  66.3 8.7 %collective-permute-done.6 = bf16[2,256,512]{2,1,0:T(8,128)(2,1)S(1)} collective-permute-done((bf16[2,256,512]{2,1,0:T(8,128)(2,1)S(1)}, bf16[2,256,512]{2,1,0:T(8,128)(2,1)S(1)}, u32[]{:S(2)}, u32[]{:S(2)}) %collective-permute-start.6) | collective-permute-done | bytes 524320 | tf_op jit(solution)/shard_map/ppermute | solution.py:126
  75.3 1.1 constant_dynamic-update-slice_fusion.12
  76.9 1.1 constant_dynamic-update-slice_fusion.4
  78.4 1.4 multiply_reduce_fusion
  79.7 1.9 copy-done.1
  81.6 1.2 fusion.37
  82.8 0.7 fusion.73
  83.6 0.5 reduce_window_sum.11
  84.1 0.8 slice_reduce_fusion
  85.4 39.3 %custom-call.3 = f32[2,1,4,1,64,64]{4,5,3,2,1,0:T(8,128)S(1)} custom-call(f32[2,1,4,1,64,64]{5,4,3,2,1,0:T(8,128)S(1)} %fusion.33), custom_call_target="InvertDiagBlocksLowerTriangular" | custom-call | tf_op jit(solution)/shard_map/vmap(vmap())/triangular_solve | solution.py:74
  124.8 3.8 %multiply_convert_fusion = bf16[2,256,128]{2,1,0:T(8,128)(2,1)S(1)} fusion(bf16[4096,128]{1,0:T(8,128)(2,1)} %param.21, bf16[2,256,8192]{2,1,0:T(8,128)(2,1)} %copy-done.1, s32[]{:T(128)S(6)} %select_n.97), kind=kOutput, calls=%fused_computation.59 | convolution fusion | flops 537198592 | bytes 5373956 | tf_op jit(solution)/shard_map/abf,fc->abc/dot_general | solution.py:133
  128.9 0.6 convolution_bitcast_fusion.3
  129.6 1.3 copy.42
  131.0 0.9 broadcast_in_dim.25
  131.9 5.6 %while.39 = (s32[]{:T(128)}, f32[2,1,128,256]{3,2,0,1:T(8,128)S(1)}, f32[4,2,1]{1,2,0:T(1,128)}, f32[4,2,1,64,128]{4,3,0,1,2:T(8,128)S(1)}, f32[4,2,1,64,256]{4,...) while((s32[]{:T(128)}, f32[2,1,128,256]{3,2,0,1:T(8,128)S(1)}, f32[4,2,1]{1,2,0:T(1,128)}, ...), condition=%wide.region_3.4_spmd, body=%wide.region_2.3_spmd.sunk | while | flops 100827136 | bytes 1312357 | solution.py:94
  132.2 0.7 fusion.119
  133.6 0.7 fusion.119
  134.2 0.4 fusion.120
  135.0 0.7 fusion.119
  135.6 0.4 fusion.120
  136.4 0.7 fusion.119
  137.5 15.8 %all-gather.2 = f32[8,1,128,128]{3,2,1,0:T(8,128)S(1)} all-gather(f32[2,1,128,128]{3,2,1,0:T(8,128)S(1)} %slice_bitcast_fusion.1), channel_id=4, replica_groups=mesh['sp'=4,'tp'=8] {'sp'}, dimensions={0}, use_global_device_ids=true | all-gather | bytes 655360 | tf_op jit(solution)/shard_map/all_gather | solution.py:36
  153.3 0.8 broadcast_in_dim.30
  154.2 1.8 while.40
  156.0 1.0 convolution_bitcast_fusion.5
  157.2 11.8 %psum.7 = f32[2,1,128]{2,0,1:T(2,128)S(1)} all-reduce(f32[2,1,128]{2,0,1:T(2,128)S(1)} %bitcast.217), channel_id=1, replica_groups=mesh['sp'=4,'tp'=8] {'sp'}, use_global_device_ids=true, to_apply=%region_11.12 | all-reduce | flops 256 | bytes 2048 | tf_op jit(solution)/shard_map/psum | solution.py:195
  169.0 1.6 multiply_reduce_fusion.1
  170.7 3.3 %convolution_bitcast_fusion.2 = f32[4096,2]{1,0:T(8,128)} fusion(bf16[128,4096]{1,0:T(8,128)(2,1)S(1)} %copy-done.3, f32[2,1,128]{2,0,1:T(2,128)S(1)} %get-tuple-element.345, f32[128]{0:T(128)} %param.28, f32[2]{0:T(128)S(1)} %add_rsqrt_fusion.1, bf16[2,4096]{1,0:T(2,128)(2,1)S(1)} %copy-done.5, bf16[4096,128]{1,0:T(8,128)(2,1)} %param.23), kind=kOutput, calls=%fused_computation.29 | convolution fusion | flops 4196352 | bytes 2147848
  173.9 14.3 %all-gather = bf16[8,1,128,128]{3,2,1,0:T(8,128)(2,1)S(1)} all-gather(bf16[2,1,128,128]{3,2,1,0:T(8,128)(2,1)S(1)} %get-tuple-element.355), channel_id=2, replica_groups=mesh['sp'=4,'tp'=8] {'sp'}, dimensions={0}, use_global_device_ids=true | all-gather | bytes 327680 | tf_op jit(solution)/shard_map/all_gather | solution.py:14
  188.2 13.8 %all-gather.1 = bf16[8,1,128,128]{3,2,1,0:T(8,128)(2,1)S(1)} all-gather(bf16[2,1,128,128]{3,2,1,0:T(8,128)(2,1)S(1)} %get-tuple-element.354), channel_id=3, replica_groups=mesh['sp'=4,'tp'=8] {'sp'}, dimensions={0}, use_global_device_ids=true | all-gather | bytes 327680 | tf_op jit(solution)/shard_map/all_gather | solution.py:14
  202.0 1.1 while.41
  203.1 0.9 fusion.36
  204.0 8.5 %reduce-scatter.4.cloned.1.call-done = f32[512,2]{1,0:T(8,128)} async-done(((f32[4096,2]{1,0:T(8,128)}), f32[512,2]{1,0:T(8,128)}) %reduce-scatter.4.cloned.1.call-update) | async-done | bytes 4112
  212.5 1.6 copy.60
  (83 shorter events, 7.3 us)
Async XLA Ops:
  7.2 32.3 %copy-start = (bf16[4096,128]{1,0:T(8,128)(2,1)S(1)}, bf16[4096,128]{1,0:T(8,128)(2,1)}, u32[]{:S(2)}) copy-start(bf16[4096,128]{1,0:T(8,128)(2,1)} %param.20) | copy-start | bytes 3145732
  7.2 69.4 %copy-start.2 = (bf16[2,256,512]{2,1,0:T(8,128)(2,1)S(1)}, bf16[2,256,512]{2,1,0:T(8,128)(2,1)}, u32[]{:S(2)}) copy-start(bf16[2,256,512]{2,1,0:T(8,128)(2,1)} %param.18) | copy-start | bytes 1572868
  7.2 205.3 %reduce-scatter.4.cloned.1.call-start = ((), (), s32[]{:S(2)}) async-start(), calls=%async_computation.1 | async-start | bytes 2359296
  7.2 10.5 %collective-permute-start = (bf16[2,256,512]{2,1,0:T(8,128)(2,1)}, bf16[2,256,512]{2,1,0:T(8,128)(2,1)S(1)}, u32[]{:S(2)}, u32[]{:S(2)}) collective-permute-start(bf16[2,256,512]{2,1,0:T(8,128)(2,1)} %param.18), channel_id=1, source_target_pairs={{0,1},{1,2},{2,3},{3,4},{4,5},{5,6},{6,7},{7,0},{8,9},{9,10},{10,1... | collective-permute-start | bytes 1572872 | tf_op jit(solution)/shard_map/ppermute | solution.py:126
  17.7 9.5 %collective-permute-start.1 = (bf16[2,256,512]{2,1,0:T(8,128)(2,1)S(1)}, bf16[2,256,512]{2,1,0:T(8,128)(2,1)S(1)}, u32[]{:S(2)}, u32[]{:S(2)}) collective-permute-start(bf16[2,256,512]{2,1,0:T(8,128)(2,1)S(1)} %collective-permute-done), channel_id=1, source_target_pairs={{0,1},{1,2},{2,3},{3,4},{4,5},{5,6},{6,7},{7,0},{8,9},{9,10},{10,1... | collective-permute-start | bytes 1572872 | tf_op jit(solution)/shard_map/ppermute | solution.py:126
  27.2 9.5 %collective-permute-start.2 = (bf16[2,256,512]{2,1,0:T(8,128)(2,1)S(1)}, bf16[2,256,512]{2,1,0:T(8,128)(2,1)S(1)}, u32[]{:S(2)}, u32[]{:S(2)}) collective-permute-start(bf16[2,256,512]{2,1,0:T(8,128)(2,1)S(1)} %collective-permute-done.1), channel_id=1, source_target_pairs={{0,1},{1,2},{2,3},{3,4},{4,5},{5,6},{6,7},{7,0},{8,9},{9,10},{10,1... | collective-permute-start | bytes 1572872 | tf_op jit(solution)/shard_map/ppermute | solution.py:126
  36.7 9.6 %collective-permute-start.3 = (bf16[2,256,512]{2,1,0:T(8,128)(2,1)S(1)}, bf16[2,256,512]{2,1,0:T(8,128)(2,1)}, u32[]{:S(2)}, u32[]{:S(2)}) collective-permute-start(bf16[2,256,512]{2,1,0:T(8,128)(2,1)S(1)} %collective-permute-done.2), channel_id=1, source_target_pairs={{0,1},{1,2},{2,3},{3,4},{4,5},{5,6},{6,7},{7,0},{8,9},{9,10},{10,1... | collective-permute-start | bytes 1572872 | tf_op jit(solution)/shard_map/ppermute | solution.py:126
  36.8 41.5 %copy-start.4 = (f32[128,128]{0,1:T(8,128)}, f32[128,128]{0,1:T(8,128)S(1)}, u32[]{:S(2)}) copy-start(f32[128,128]{0,1:T(8,128)S(1)} %fusion.64) | copy-start | bytes 196612
  46.3 9.7 %collective-permute-start.4 = (bf16[2,256,512]{2,1,0:T(8,128)(2,1)}, bf16[2,256,512]{2,1,0:T(8,128)(2,1)S(1)}, u32[]{:S(2)}, u32[]{:S(2)}) collective-permute-start(bf16[2,256,512]{2,1,0:T(8,128)(2,1)} %collective-permute-done.3), channel_id=1, source_target_pairs={{0,1},{1,2},{2,3},{3,4},{4,5},{5,6},{6,7},{7,0},{8,9},{9,10},{10,1... | collective-permute-start | bytes 1572872 | tf_op jit(solution)/shard_map/ppermute | solution.py:126
  46.5 19.0 %copy-start.7 = (f32[2]{0:T(128)}, f32[2]{0:T(128)S(1)}, u32[]{:S(2)}) copy-start(f32[2]{0:T(128)S(1)} %multiply_reduce_fusion.2) | copy-start | bytes 28
  56.1 9.5 %collective-permute-start.5 = (bf16[2,256,512]{2,1,0:T(8,128)(2,1)S(1)}, bf16[2,256,512]{2,1,0:T(8,128)(2,1)S(1)}, u32[]{:S(2)}, u32[]{:S(2)}) collective-permute-start(bf16[2,256,512]{2,1,0:T(8,128)(2,1)S(1)} %collective-permute-done.4), channel_id=1, source_target_pairs={{0,1},{1,2},{2,3},{3,4},{4,5},{5,6},{6,7},{7,0},{8,9},{9,10},{10,1... | collective-permute-start | bytes 1572872 | tf_op jit(solution)/shard_map/ppermute | solution.py:126
  57.0 8.6 %copy-start.8 = (f32[2]{0:T(128)}, f32[2]{0:T(128)S(1)}, u32[]{:S(2)}) copy-start(f32[2]{0:T(128)S(1)} %get-tuple-element.362) | copy-start | bytes 28
  65.6 9.5 %collective-permute-start.6 = (bf16[2,256,512]{2,1,0:T(8,128)(2,1)S(1)}, bf16[2,256,512]{2,1,0:T(8,128)(2,1)S(1)}, u32[]{:S(2)}, u32[]{:S(2)}) collective-permute-start(bf16[2,256,512]{2,1,0:T(8,128)(2,1)S(1)} %collective-permute-done.5), channel_id=1, source_target_pairs={{0,1},{1,2},{2,3},{3,4},{4,5},{5,6},{6,7},{7,0},{8,9},{9,10},{10,1... | collective-permute-start | bytes 1572872 | tf_op jit(solution)/shard_map/ppermute | solution.py:126
  76.8 5.9 %copy-start.6 = (f32[2,256,1]{1,2,0:T(1,128)S(1)}, f32[2,256,1]{1,2,0:T(1,128)}, u32[]{:S(2)}) copy-start(f32[2,256,1]{1,2,0:T(1,128)} %param.27) | copy-start | bytes 6148
  78.3 3.2 %copy-start.1 = (bf16[2,256,8192]{2,1,0:T(8,128)(2,1)}, bf16[2,256,8192]{2,1,0:T(8,128)(2,1)S(1)}, u32[]{:S(2)}) copy-start(bf16[2,256,8192]{2,1,0:T(8,128)(2,1)S(1)} %constant_dynamic-update-slice_fusion) | copy-start | bytes 25165828
  128.6 40.4 %copy-start.5 = (bf16[2,4096]{1,0:T(2,128)(2,1)S(1)}, bf16[2,4096]{1,0:T(2,128)(2,1)}, u32[]{:S(2)}) copy-start(bf16[2,4096]{1,0:T(2,128)(2,1)} %param.19) | copy-start | bytes 49156
  128.9 41.8 %copy-start.3 = (bf16[128,4096]{1,0:T(8,128)(2,1)S(1)}, bf16[128,4096]{1,0:T(8,128)(2,1)}, u32[]{:S(2)}) copy-start(bf16[128,4096]{1,0:T(8,128)(2,1)} %param.29) | copy-start | bytes 3145732
Sparse Core Ops, SparseCore 0:
  174.1 38.3 reduce-scatter.3
